TPU v7x, 32 devices: a whole 2x2x4 slice. The times are simulated.
32 devices in a mesh: sp: 16 (over z, y, x), tp: 2 (over core).
Axes of the slice: x: 2, y: 2, z: 4, core: 2. Of those that a mesh axis runs over, the one named last changes fastest.
Arguments:
- resid: bfloat16 [6144, 2048], P('sp'), may hold values from -6 to 6
- x_branch: bfloat16 [6144, 2048], P('sp', 'tp'), may hold values from -6 to 6
- gate_branch: bfloat16 [6144, 2048], P('sp', 'tp'), may hold values from -6 to 6
- conv_w: float32 [4, 2048], P(None, 'tp'), may hold values from -3 to 3
- gate_a_w: bfloat16 [32, 64, 64], P('tp'), may hold values from -0.75 to 0.75
- gate_x_w: bfloat16 [32, 64, 64], P('tp'), may hold values from -0.75 to 0.75
- decay_rate: float32 [2048], P('tp'), may hold values from 0 to 0.01, as said below
- decay_extra: float32 [6144, 2048], P('sp', 'tp'), may hold values from -3 to 0, as said below
- w_proj: bfloat16 [2048, 2048], P('tp'), may hold values from -0.125 to 0.125
- mix_gain: float32 [2048], replicated, may hold values from 0.1 to 1.9
- pre_gain: float32 [2048], replicated, may hold values from 0.1 to 1.9
- w_gate: bfloat16 [2048, 5632], P('sp', 'tp'), may hold values from -0.125 to 0.125
- w_up: bfloat16 [2048, 5632], P('sp', 'tp'), may hold values from -0.125 to 0.125
- w_down: bfloat16 [5632, 2048], P('tp', 'sp'), may hold values from -0.078125 to 0.078125
- out_gain: float32 [2048], replicated, may hold values from 0.1 to 1.9
Outputs:
- stream_out: bfloat16 [6144, 2048], P(('sp', 'tp'))
Inputs may be any that keep to these rules, and one draw needn't show every extreme that they name: `decay_rate`: positive rates. `decay_extra`: non-positive values.
All inputs are finite; a program needn't handle non-finite values.
Results may differ from a plain program's by a relative error of at most 0.015.
Values may be sent and summed in bfloat16 or wider, within the bound.
No kernel may reach another device: no remote copies, remote signals or barrier semaphores. Data moves between devices by JAX's collectives and lax.ppermute only.
A program may use at most 128 MiB of HBM per device.

v0:
```python
import jax
import jax.numpy as jnp
from jax import lax
from jax.sharding import PartitionSpec as P

LRU_SCALE = 8.0
NORM_EPS = 1e-06


def from_behind(value, axis, steps):
    count = lax.axis_size(axis)
    first, last = (max(0, -steps), min(count, count - steps))
    return lax.ppermute(value, axis, [(source, source + steps) for source in range(first, last)])


def prefix(part, axis, combine, identity):
    place = lax.axis_index(axis)
    gathered = jax.tree.map(lambda a: lax.all_gather(a, axis), part)
    state = jax.tree.map(lambda a, e: jnp.zeros_like(a) + jnp.asarray(e, a.dtype), part, identity)

    def one(turn, state):
        return combine(
            state, jax.tree.map(lambda a: lax.dynamic_index_in_dim(a, turn, 0, False), gathered)
        )

    return lax.fori_loop(0, place, one, state)


def chain(earlier, later):
    return (earlier[0] * later[0], later[0] * earlier[1] + later[1])


def rms_scale(values, gains):
    return values * lax.rsqrt(jnp.mean(values * values, axis=-1, keepdims=True) + NORM_EPS) * gains


def shards(
    resid,
    x_branch,
    gate_branch,
    conv_w,
    gate_a_w,
    gate_x_w,
    decay_rate,
    decay_extra,
    w_proj,
    mix_gain,
    pre_gain,
    w_gate,
    w_up,
    w_down,
    out_gain,
):
    length = x_branch.shape[0]
    width = x_branch.shape[1]
    taps = conv_w.shape[0]
    before = from_behind(x_branch[length - (taps - 1) :], "sp", 1)
    padded = jnp.concatenate([before, x_branch], axis=0).astype(jnp.float32)
    conv = padded[0:length] * conv_w[0]
    for tap in range(1, taps):
        conv = conv + padded[tap : tap + length] * conv_w[tap]
    conv_out = conv.astype(jnp.bfloat16)
    nblocks = gate_a_w.shape[0]
    grouped = conv_out.reshape(length, nblocks, gate_a_w.shape[1])
    recur = jax.nn.sigmoid(
        jnp.einsum("rnc,ncd->rnd", grouped, gate_a_w, preferred_element_type=jnp.float32).reshape(
            length, width
        )
    )
    inject = jax.nn.sigmoid(
        jnp.einsum("rnc,ncd->rnd", grouped, gate_x_w, preferred_element_type=jnp.float32).reshape(
            length, width
        )
    )
    log_decay = -LRU_SCALE * recur * decay_rate + decay_extra
    decay = jnp.exp(log_decay)
    drive = jnp.sqrt(-jnp.expm1(2.0 * log_decay)) * inject * conv_out.astype(jnp.float32)
    prod_local, state_local = lax.associative_scan(chain, (decay, drive), axis=0)
    identity = (jnp.ones((width,), jnp.float32), jnp.zeros((width,), jnp.float32))
    carried = prefix((prod_local[-1], state_local[-1]), "sp", chain, identity)
    state = state_local + prod_local * carried[1][None, :]
    mixer = (state * jax.nn.gelu(gate_branch.astype(jnp.float32))).astype(jnp.bfloat16)
    share_rows = length // lax.axis_size("tp")
    first = lax.axis_index("tp") * share_rows
    mixed = lax.psum(
        jnp.dot(mixer, w_proj, preferred_element_type=jnp.float32).astype(jnp.bfloat16), "tp"
    ).astype(jnp.float32)
    stream = resid.astype(jnp.float32) + rms_scale(mixed, mix_gain)
    normed = rms_scale(stream, pre_gain).astype(jnp.bfloat16)
    after_mix = lax.dynamic_slice_in_dim(stream, first, share_rows, 0)
    gate_full, up_full = (
        lax.all_gather(w_gate, "sp", axis=0, tiled=True),
        lax.all_gather(w_up, "sp", axis=0, tiled=True),
    )
    down_full = lax.all_gather(w_down, "sp", axis=1, tiled=True)
    gate = jnp.dot(normed, gate_full, preferred_element_type=jnp.float32)
    upward = jnp.dot(normed, up_full, preferred_element_type=jnp.float32)
    hidden = (jax.nn.silu(gate) * upward).astype(jnp.bfloat16)
    ffn = lax.psum_scatter(
        jnp.dot(hidden, down_full, preferred_element_type=jnp.float32).astype(jnp.bfloat16),
        "tp",
        scatter_dimension=0,
        tiled=True,
    ).astype(jnp.float32)
    return (after_mix + 0.5 * rms_scale(ffn, out_gain)).astype(jnp.bfloat16)


def solution(mesh):
    return jax.shard_map(
        shards,
        mesh=mesh,
        in_specs=(
            P("sp", None),
            P("sp", "tp"),
            P("sp", "tp"),
            P(None, "tp"),
            P("tp", None, None),
            P("tp", None, None),
            P("tp"),
            P("sp", "tp"),
            P("tp", None),
            P(),
            P(),
            P("sp", "tp"),
            P("sp", "tp"),
            P("tp", "sp"),
            P(),
        ),
        out_specs=P(("sp", "tp"), None),
        check_vma=False,
    )
```

profile of v0, /device:TPU:0, one launch (start us, length us, event | category | flops | bytes accessed | tf_op | source)
XLA Modules:
  0.0 737.7 jit_solution(13793167642620603508)
XLA Ops:
  8.1 4.9 collective-permute-start
  14.6 1.4 maximum_convert_fusion
  17.8 1.8 add_divide_fusion.1
  19.6 1.7 copy.106
  21.3 1.8 add_divide_fusion
  23.0 1.6 copy.108
  24.6 5.3 convert_multiply_fusion.7
  30.0 4.5 slice.281
  34.4 2.1 slice.282
  36.6 2.1 slice.280
  38.7 2.2 slice.284
  40.9 3.4 multiply_add_fusion.2
  44.2 2.7 slice.287
  46.9 2.7 slice.288
  49.6 2.7 slice.286
  52.4 2.7 slice.290
  55.1 2.4 multiply_add_fusion.3
  57.4 1.7 slice.293
  59.1 1.7 slice.294
  60.8 1.7 slice.292
  62.5 1.7 slice.296
  64.1 2.0 multiply_add_fusion.4
  67.4 1.6 slice.298
  69.0 1.6 slice.302
  70.6 1.7 multiply_add_fusion.5
  73.6 1.5 slice.304
  75.1 1.5 slice.308
  76.6 1.6 multiply_add_fusion.6
  79.4 1.5 slice.310
  80.9 1.5 slice.314
  82.3 1.4 multiply_add_fusion.7
  84.5 1.4 slice.318
  87.8 1.4 slice.326
  89.1 1.3 slice.366
  94.5 1.5 slice.303
  96.6 1.4 slice.390
  102.2 1.7 slice.291
  103.9 1.7 slice.334
  106.9 1.4 slice.362
  108.2 2.7 slice.285
  111.0 2.8 slice.336
  113.8 1.4 slice.361
  115.1 1.4 slice.387
  116.5 2.3 slice.279
  118.8 2.2 slice.338
  128.0 3.1 pad.113
  134.1 1.4 fusion.21
  135.6 3.2 pad.112
  139.6 42.0 %all-gather.1 = f32[16,1,1024]{2,1,0:T(1,128)S(1)} all-gather(f32[1,1,1024]{2,1,0:T(1,128)S(1)} %add_bitcast_fusion), channel_id=1, replica_groups=mesh['sp'=16,'tp'=2] {'sp'}, dimensions={0}, use_global_device_ids=true | all-gather | bytes 69632 | tf_op jit(solution)/shard_map/all_gather | solution.py:18
  181.7 3.1 pad.129
  184.9 3.2 pad.128
  188.9 35.8 %all-gather = f32[16,1,1024]{2,1,0:T(1,128)S(1)} all-gather(f32[1,1,1024]{2,1,0:T(1,128)S(1)} %add_bitcast_fusion.1), channel_id=1, replica_groups=mesh['sp'=16,'tp'=2] {'sp'}, dimensions={0}, use_global_device_ids=true | all-gather | bytes 69632 | tf_op jit(solution)/shard_map/all_gather | solution.py:18
  224.7 7.0 convolution_convert_fusion.1
  233.6 17.4 %all-reduce.34.cloned.1.call-done = bf16[384,2048]{1,0:T(8,128)(2,1)} async-done(((bf16[384,2048]{1,0:T(8,128)(2,1)}), bf16[384,2048]{1,0:T(8,128)(2,1)}) %all-reduce.34.cloned.1.call-update) | async-done | bytes 1572880 | tf_op jit(solution)/shard_map/psum | solution.py:85
  250.9 1.9 fusion.1
  252.9 2.3 multiply_reduce_fusion
  255.2 119.6 %all-gather.6.cloned.1.call-done = bf16[2048,2816]{1,0:T(8,128)(2,1)} async-done(((bf16[128,2816]{1,0:T(8,128)(2,1)}), bf16[2048,2816]{1,0:T(8,128)(2,1)}) %all-gather.6.cloned.1.call-update) | async-done | bytes 11534352 | tf_op jit(solution)/shard_map/all_gather | solution.py:92
  374.9 9.6 %fusion.43 = f32[384,2816]{1,0:T(8,128)} fusion(bf16[2048,2816]{1,0:T(8,128)(2,1)} %all-gather.6.cloned.1.call-done, f32[384,2048]{1,0:T(8,128)S(1)} %get-tuple-element.61, f32[2048]{0:T(1024)S(1)} %copy-done.38, f32[384]{0:T(512)S(1)} %add_rsqrt_fusion), kind=kOutput, calls=%fused_computation.118 | convolution fusion | flops 4431544320 | bytes 19015168 | tf_op jit(solution)/shard_map/dot_general | solution.py:96
  384.4 173.1 %all-gather.10.cloned.1.call-done = bf16[2816,2048]{1,0:T(8,128)(2,1)} async-done(((bf16[2816,128]{1,0:T(8,128)(2,1)}), bf16[2816,2048]{1,0:T(8,128)(2,1)}) %all-gather.10.cloned.1.call-update) | async-done | bytes 11534352 | tf_op jit(solution)/shard_map/all_gather | solution.py:95
  557.5 142.0 %all-gather.8.cloned.1.call-done = bf16[2048,2816]{1,0:T(8,128)(2,1)} async-done(((bf16[128,2816]{1,0:T(8,128)(2,1)}), bf16[2048,2816]{1,0:T(8,128)(2,1)}) %all-gather.8.cloned.1.call-update) | async-done | bytes 11534352 | tf_op jit(solution)/shard_map/all_gather | solution.py:93
  699.5 19.3 %convolution_convert_fusion = bf16[384,2048]{1,0:T(8,128)(2,1)} fusion(bf16[2816,2048]{1,0:T(8,128)(2,1)} %all-gather.10.cloned.1.call-done, bf16[2048,2816]{1,0:T(8,128)(2,1)} %all-gather.8.cloned.1.call-done, f32[384,2816]{1,0:T(8,128)} %fusion.43, f32[384,2048]{1,0:T(8,128)S(1)} %get-tuple-element.61, f32[2048]{0:T(1024)S(1)} %copy-done.38, ...), kind=kOutput, calls=%fused_computation.12 | convolution fusion | flops 8868003840 | bytes 32122368 | tf_op jit(solution)/shard_map/dot_general | solution.py:100
  718.9 7.4 reduce-scatter.2.cloned.1.call-done
  726.3 1.4 fusion.4
  727.7 2.4 fusion.8
  (189 shorter events, 33.9 us)
Async XLA Ops:
  7.4 10.4 %copy-start = (bf16[16,64,64]{2,1,0:T(8,128)(2,1)S(1)}, bf16[16,64,64]{2,1,0:T(8,128)(2,1)}, u32[]{:S(2)}) copy-start(bf16[16,64,64]{2,1,0:T(8,128)(2,1)} %param.21) | copy-start | bytes 393220
  7.4 243.6 %all-reduce.34.cloned.1.call-start = ((), (), s32[]{:S(2)}) async-start(), calls=%async_computation.1 | async-start | bytes 3145728 | tf_op jit(solution)/shard_map/psum | solution.py:85
  8.1 6.5 collective-permute-start
  19.6 1.7 copy-start.37
  29.9 4.5 copy-start.2
  116.5 5.7 copy-start.15
  116.5 5.7 copy-start.16
  116.5 5.7 copy-start.17
  116.5 6.0 copy-start.18
  116.5 6.0 copy-start.19
  116.5 6.0 copy-start.26
  116.5 6.0 copy-start.27
  118.8 3.8 copy-start.14
  118.8 3.9 copy-start.33
  118.8 3.9 copy-start.32
  121.6 2.1 copy-start.31
  122.2 1.6 copy-start.30
  122.6 1.3 copy-start.13
  122.8 1.2 copy-start.29
  123.7 0.7 copy-start.28
  124.0 0.9 copy-start.11
  124.0 1.0 copy-start.12
  124.5 0.7 copy-start.25
  125.0 0.7 copy-start.24
  125.7 1.0 copy-start.9
  125.7 1.2 copy-start.10
  126.9 0.7 copy-start.23
  128.0 3.1 copy-start.22
  132.5 1.4 copy-start.4
  132.5 1.6 copy-start.5
  134.1 1.4 copy-start.21
  135.6 3.2 copy-start.8
  135.6 46.1 %copy-start.7 = (f32[192,1024]{1,0:T(8,128)S(1)}, f32[192,1024]{1,0:T(8,128)}, u32[]{:S(2)}) copy-start(f32[192,1024]{1,0:T(8,128)} %add.291) | copy-start | bytes 2359300
  138.8 46.0 %copy-start.6 = (f32[191,1024]{1,0:T(8,128)S(1)}, f32[191,1024]{1,0:T(8,128)}, u32[]{:S(2)}) copy-start(f32[191,1024]{1,0:T(8,128)} %get-tuple-element.71) | copy-start | bytes 2347012
  138.8 46.0 %copy-start.20 = (f32[1,1024]{1,0:T(1,128)S(1)}, f32[1,1024]{1,0:T(1,128)}, u32[]{:S(2)}) copy-start(f32[1,1024]{1,0:T(1,128)} %slice.386) | copy-start | bytes 12292
  184.9 39.8 %copy-start.36 = (bf16[384,1024]{1,0:T(8,128)(2,1)S(1)}, bf16[384,1024]{1,0:T(8,128)(2,1)}, u32[]{:S(2)}) copy-start(bf16[384,1024]{1,0:T(8,128)(2,1)} %param.19) | copy-start | bytes 2359300
  231.8 143.1 %all-gather.6.cloned.1.call-start = ((), (), s32[]{:S(2)}) async-start(), calls=%async_computation.2 | async-start | bytes 12255232 | tf_op jit(solution)/shard_map/all_gather | solution.py:92
  232.3 20.5 %copy-start.34 = (f32[2048]{0:T(1024)S(1)}, f32[2048]{0:T(1024)}, u32[]{:S(2)}) copy-start(f32[2048]{0:T(1024)} %param.26) | copy-start | bytes 24580
  232.3 325.2 %all-gather.10.cloned.1.call-start = ((), (), s32[]{:S(2)}) async-start(), calls=%async_computation.4 | async-start | bytes 12255232 | tf_op jit(solution)/shard_map/all_gather | solution.py:95
  232.9 466.6 %all-gather.8.cloned.1.call-start = ((), (), s32[]{:S(2)}) async-start(), calls=%async_computation.3 | async-start | bytes 12255232 | tf_op jit(solution)/shard_map/all_gather | solution.py:93
  233.5 492.8 %reduce-scatter.2.cloned.1.call-start = ((), (), s32[]{:S(2)}) async-start(), calls=%async_computation.5 | async-start | bytes 2359296 | tf_op jit(solution)/shard_map/reduce_scatter | solution.py:99
  250.9 1.9 copy-start.3
  252.9 122.0 %copy-start.38 = (f32[2048]{0:T(1024)S(1)}, f32[2048]{0:T(1024)}, u32[]{:S(2)}) copy-start(f32[2048]{0:T(1024)} %param.27) | copy-start | bytes 24580
  718.9 8.8 %copy-start.35 = (f32[2048]{0:T(1024)S(1)}, f32[2048]{0:T(1024)}, u32[]{:S(2)}) copy-start(f32[2048]{0:T(1024)} %param.31) | copy-start | bytes 24580
  727.7 2.4 copy-start.1
Sparse Core Ops, SparseCore 0:
  231.9 19.0 all-reduce.33
  719.0 7.2 reduce-scatter.1
Sparse Core Ops, SparseCore 1:
  235.0 139.8 all-gather.5
  377.4 180.0 all-gather.9
  560.1 139.3 all-gather.7
where the time goes:
time: 740 us; the launch traced here: 738 us
  waiting for transfers between devices  461 us (62%)
  local copies, waits for them, and re-layouts  103 us (14%)
  blocking collectives  77.8 us (11%)
  matrix products  39.4 us (5%)
  other arithmetic  35.2 us (5%)
  between operations  15.9 us (2%)
    all_gather x1, waiting for transfers between devices, shards(): down_full = lax.all_gather(w_down, 'sp', axis=1, tiled=True)  173 us
    all_gather x1, waiting for transfers between devices, shards(): lax.all_gather(w_up, 'sp', axis=0, tiled=True)  142 us
    all_gather x1, waiting for transfers between devices, shards(): lax.all_gather(w_gate, 'sp', axis=0, tiled=True)  120 us
    slice x56, local copies, waits for them, and re-layouts, shards(): lax.associative_scan(chain, (decay, drive), axis=0)  79.8 us
    all_gather x2, blocking collectives, prefix(): gathered = jax.tree.map(lambda a: lax.all_gather(a, axis), part)  77.8 us
    dot_general x1, matrix products, shards(): jnp.dot(hidden, down_full, preferred_element_type=jnp.float32)  19.3 us
    psum x1, waiting for transfers between devices, shards(): lax.psum(jnp.dot(mixer, w_proj, preferred_element_type=jnp.float32).astyp...  17.4 us
    add x15, other arithmetic, chain(): return (earlier[0] * later[0], later[0] * earlier[1] + later[1])  15 us
  transfers between devices with their start and end apart: 6, of which 5 were waited for; matrix products, arithmetic and copies ran while one was open for 2% of the time, Pallas kernels for 0%

commit v1 on v0

v1 whole, which is shorter than its diff:
```python
import jax
import jax.numpy as jnp
from jax import lax
from jax.experimental import pallas as pl
from jax.experimental.pallas import tpu as pltpu
from jax.sharding import Mesh, PartitionSpec as P

LRU_SCALE = 8.0
NORM_EPS = 1e-06


def chain(earlier, later):
    return (earlier[0] * later[0], later[0] * earlier[1] + later[1])


def rms_scale(values, gains):
    return values * lax.rsqrt(jnp.mean(values * values, axis=-1, keepdims=True) + NORM_EPS) * gains


def one_minus_exp(y):
    series = 1.0
    for n in (8, 7, 6, 5, 4, 3, 2):
        series = 1.0 + y * (1.0 / n) * series
    return jnp.where(y > -0.35, -y * series, 1.0 - jnp.exp(y))


def rows_down(a, k, fill, row):
    if k % 8 == 0:
        return jnp.concatenate([jnp.full((k, a.shape[1]), fill, a.dtype), a[:-k]], axis=0)
    return jnp.where(row >= k, pltpu.roll(a, k, 0), fill)


def recur_kernel(x, before, gate, taps, wa, wx, rate, extra, u_out, v_out, last_out):
    length, lanes = x.shape
    ntaps = taps.shape[0]
    row = lax.broadcasted_iota(jnp.int32, (length, lanes), 0)
    xf = x[...].astype(jnp.float32)
    prev = before[...].astype(jnp.float32)
    conv = None
    for tap in range(ntaps):
        k = ntaps - 1 - tap
        moved = xf
        if k:
            moved = pltpu.roll(xf, k, 0)
            for r in range(k):
                at = prev.shape[0] - k + r
                moved = jnp.where(row == r, prev[at : at + 1], moved)
        term = moved * taps[tap : tap + 1]
        conv = term if conv is None else conv + term
    conv_out = conv.astype(jnp.bfloat16)
    recur = 1.0 / (1.0 + jnp.exp(-jnp.dot(conv_out, wa[0], preferred_element_type=jnp.float32)))
    inject = 1.0 / (1.0 + jnp.exp(-jnp.dot(conv_out, wx[0], preferred_element_type=jnp.float32)))
    log_decay = -LRU_SCALE * recur * rate[...] + extra[...]
    decay = jnp.exp(log_decay)
    left = one_minus_exp(2.0 * log_decay)
    root = jnp.where(left > 0.0, left * lax.rsqrt(left), 0.0)
    drive = root * inject * conv_out.astype(jnp.float32)
    k = 1
    while k < length:
        drive = drive + decay * rows_down(drive, k, 0.0, row)
        decay = decay * rows_down(decay, k, 1.0, row)
        k *= 2
    g = jax.nn.gelu(gate[...].astype(jnp.float32))
    u_out[...] = drive * g
    v_out[...] = decay * g
    last_out[0:1] = decay[length - 1 : length]
    last_out[1:2] = drive[length - 1 : length]


def pair_blocks(w, per):
    n, b, _ = w.shape
    eye = jnp.eye(per, dtype=w.dtype)
    wide = w.reshape(n // per, per, b, 1, b) * eye[None, :, None, :, None]
    return wide.reshape(n // per, per * b, per * b)


def recurrence(x, before, gate, taps, wa, wx, rate, extra):
    length, width = x.shape
    b = wa.shape[1]
    per = max(1, min(128, width) // b)
    lanes = per * b
    col = lambda i: (0, i)
    blk = lambda i: (i, 0, 0)
    return pl.pallas_call(
        recur_kernel,
        grid=(width // lanes,),
        in_specs=[
            pl.BlockSpec((length, lanes), col),
            pl.BlockSpec((before.shape[0], lanes), col),
            pl.BlockSpec((length, lanes), col),
            pl.BlockSpec((taps.shape[0], lanes), col),
            pl.BlockSpec((1, lanes, lanes), blk),
            pl.BlockSpec((1, lanes, lanes), blk),
            pl.BlockSpec((1, lanes), col),
            pl.BlockSpec((length, lanes), col),
        ],
        out_specs=[
            pl.BlockSpec((length, lanes), col),
            pl.BlockSpec((length, lanes), col),
            pl.BlockSpec((2, lanes), col),
        ],
        out_shape=[
            jax.ShapeDtypeStruct((length, width), jnp.float32),
            jax.ShapeDtypeStruct((length, width), jnp.float32),
            jax.ShapeDtypeStruct((2, width), jnp.float32),
        ],
        compiler_params=pltpu.CompilerParams(dimension_semantics=("arbitrary",)),
        name="recurrence",
    )(x, before, gate, taps, pair_blocks(wa, per), pair_blocks(wx, per), rate[None], extra)


def turn(value, axis, k):
    n = lax.axis_size(axis)
    return lax.ppermute(value, axis, [(s, (s + k) % n) for s in range(n)])


def exclusive(part, axis):
    place = lax.axis_index(axis)
    none = jnp.stack([jnp.ones_like(part[0]), jnp.zeros_like(part[1])])
    got = none
    n = lax.axis_size(axis)
    sent = [(k, turn(part, axis, k)) for k in range(1, n)]
    for k, p in reversed(sent):
        p = jnp.where(place >= k, p, none)
        got = jnp.stack(chain(got, p))
    return got


def from_peers(part, halves):
    if halves == 2:
        rows = part.shape[0] // 2
        return part[:rows].astype(jnp.float32) + turn(part[rows:], "tp", 1).astype(jnp.float32)
    return lax.psum_scatter(part, "tp", scatter_dimension=0, tiled=True).astype(jnp.float32)


def with_peers(own, halves):
    if halves == 2:
        return jnp.concatenate([own, turn(own, "tp", 1)], axis=0)
    return lax.all_gather(own, "tp", axis=0, tiled=True)


def exchange(pieces, place, n):
    got = jnp.stack(
        [
            lax.dynamic_index_in_dim(pieces, place, 0, False)
            if k == 0
            else turn(lax.dynamic_index_in_dim(pieces, (place + k) % n, 0, False), "so", k)
            for k in range(n)
        ]
    )
    order = (place - jnp.arange(n)) % n
    return jnp.take(got, order, axis=0)


def shards(
    resid,
    x_branch,
    gate_branch,
    conv_w,
    gate_a_w,
    gate_x_w,
    decay_rate,
    decay_extra,
    w_proj,
    mix_gain,
    pre_gain,
    w_gate,
    w_up,
    w_down,
    out_gain,
):
    no, ni, nt = (lax.axis_size(a) for a in ("so", "si", "tp"))
    o, t = lax.axis_index("so"), lax.axis_index("tp")
    length = x_branch.shape[0]
    taps = conv_w.shape[0]
    share = length // nt
    width = resid.shape[1]

    r, f = w_gate.shape
    fs = f // no
    cut = jnp.stack([w_gate.reshape(r, no, fs), w_up.reshape(r, no, fs)], axis=2)
    cut = cut.reshape(r, no, 2 * fs).transpose(1, 0, 2)
    wide = exchange(cut, o, no).reshape(no * r, 2 * fs)
    wide = lax.all_gather(wide, "si", axis=0, tiled=True)
    tall = exchange(w_down.reshape(no, fs, r), o, no).reshape(no * fs, r)
    tall = lax.all_gather(tall, "si", axis=0, tiled=True)
    tall = tall.reshape(ni, no, fs, r).transpose(2, 1, 0, 3).reshape(fs, width)

    n_sp = no * ni
    before = lax.ppermute(
        x_branch[length - (taps - 1) :], ("so", "si"), [(s, s + 1) for s in range(n_sp - 1)]
    )
    u, v, last = recurrence(
        x_branch, before, gate_branch, conv_w, gate_a_w, gate_x_w, decay_rate, decay_extra
    )
    inner = exclusive(last, "si")
    whole = jnp.stack(chain(inner, last))
    total = jnp.where(lax.axis_index("si") == ni - 1, whole, 0.0)
    total = sum([total] + [turn(total, "si", k) for k in range(1, ni)])
    outer = exclusive(total, "so")
    carried = chain(outer, inner)[1]
    mixer = (u + v * carried[None, :]).astype(jnp.bfloat16)
    part = jnp.dot(mixer, w_proj, preferred_element_type=jnp.float32).astype(jnp.bfloat16)
    if nt == 2:
        part = part.reshape(2, share, width)
        part = jnp.concatenate(
            [lax.dynamic_index_in_dim(part, t, 0, False), lax.dynamic_index_in_dim(part, 1 - t, 0, False)]
        )
    mixed = from_peers(part, nt)
    own = lax.dynamic_slice_in_dim(resid, t * share, share, 0).astype(jnp.float32)
    stream = own + rms_scale(mixed, mix_gain)
    normed = rms_scale(stream, pre_gain).astype(jnp.bfloat16)
    normed = normed.reshape(share, no, ni, r).transpose(0, 2, 1, 3).reshape(share, width)

    def forward(rows):
        both = jnp.dot(rows, wide, preferred_element_type=jnp.float32)
        hidden = (jax.nn.silu(both[:, :fs]) * both[:, fs:]).astype(jnp.bfloat16)
        return jnp.dot(hidden, tall, preferred_element_type=jnp.float32).astype(jnp.bfloat16)

    order = sorted(range(no), key=lambda k: -min(k, no - k))
    rows = {k: with_peers(turn(normed, "so", k) if k else normed, nt) for k in order}
    ffn = None
    for k in order:
        piece = from_peers(forward(rows[k]), nt)
        if k:
            piece = turn(piece.astype(jnp.bfloat16), "so", no - k).astype(jnp.float32)
        ffn = piece if ffn is None else ffn + piece
    return (stream + 0.5 * rms_scale(ffn, out_gain)).astype(jnp.bfloat16)


def solution(mesh):
    n_sp, n_tp = mesh.shape["sp"], mesh.shape["tp"]
    inner = next(k for k in (4, 2, 1) if n_sp % k == 0)
    cut = Mesh(mesh.devices.reshape(n_sp // inner, inner, n_tp), ("so", "si", "tp"))
    sp = ("so", "si")
    return jax.shard_map(
        shards,
        mesh=cut,
        in_specs=(
            P(sp, None),
            P(sp, "tp"),
            P(sp, "tp"),
            P(None, "tp"),
            P("tp", None, None),
            P("tp", None, None),
            P("tp"),
            P(sp, "tp"),
            P("tp", None),
            P(),
            P(),
            P(sp, "tp"),
            P(sp, "tp"),
            P("tp", sp),
            P(),
        ),
        out_specs=P(("so", "si", "tp"), None),
        check_vma=False,
    )
```

time: 740 us -> 312 us (0.42)
  the two profiles are of different devices: /device:TPU:0 before, /device:TPU:11 now
where the time goes in v1:
time: 312 us; the launch traced here: 311 us
  waiting for transfers between devices  187 us (60%)
  starting transfers between devices  33.4 us (11%)
  matrix products  28.4 us (9%)
  local copies, waits for them, and re-layouts  25.7 us (8%)
  between operations  13.9 us (4%)
  other arithmetic  12 us (4%)
  Pallas kernels  10.3 us (3%)
    ppermute x30, waiting for transfers between devices, turn(): return lax.ppermute(value, axis, [(s, (s + k) % n) for s in range(n)])  187 us
    ppermute x30, starting transfers between devices, turn(): return lax.ppermute(value, axis, [(s, (s + k) % n) for s in range(n)])  30.3 us
    dot_general x4, matrix products, forward(): both = jnp.dot(rows, wide, preferred_element_type=jnp.float32)  17.5 us
    pallas_call x1, Pallas kernels, recurrence(): pl.pallas_call(recur_kernel, grid=(width // lanes,), in_specs=[pl.BlockSp...  10.3 us
  transfers between devices with their start and end apart: 33, of which 21 were waited for; matrix products, arithmetic and copies ran while one was open for 18% of the time, Pallas kernels for 3%

profile of v1, /device:TPU:11, one launch (start us, length us, event | category | flops | bytes accessed | tf_op | source)
XLA Modules:
  0.0 310.7 jit_solution(15438595952678096778)
XLA Ops:
  6.5 1.2 constant_dynamic-slice_fusion
  7.8 1.3 collective-permute-start.16
  9.1 1.1 collective-permute-start.17
  10.2 1.4 collective-permute-start.18
  11.8 1.4 collective-permute-done.16
  13.3 10.7 %collective-permute-done.17 = bf16[704,128]{1,0:T(8,128)(2,1)S(1)} collective-permute-done((bf16[704,128]{1,0:T(8,128)(2,1)S(1)}, bf16[704,128]{1,0:T(8,128)(2,1)S(1)}, u32[]{:S(2)}, u32[]{:S(2)}) %collective-permute-start.17) | collective-permute-done | bytes 180256 | tf_op jit(solution)/shard_map/ppermute | solution.py:114
  23.9 2.8 collective-permute-done.18
  26.8 0.7 gather_fusion.1
  27.6 2.2 bitcast_select_fusion.1
  32.0 1.5 collective-permute-start.15
  33.8 7.0 %collective-permute-done.13 = bf16[128,1408]{1,0:T(8,128)(2,1)S(1)} collective-permute-done((bf16[128,1408]{1,0:T(8,128)(2,1)S(1)}, bf16[128,1408]{1,0:T(8,128)(2,1)S(1)}, u32[]{:S(2)}, u32[]{:S(2)}) %collective-permute-start.13) | collective-permute-done | bytes 360480 | tf_op jit(solution)/shard_map/ppermute | solution.py:114
  40.8 21.2 %collective-permute-done.14 = bf16[128,1408]{1,0:T(8,128)(2,1)S(1)} collective-permute-done((bf16[128,1408]{1,0:T(8,128)(2,1)S(1)}, bf16[128,1408]{1,0:T(8,128)(2,1)S(1)}, u32[]{:S(2)}, u32[]{:S(2)}) %collective-permute-start.14) | collective-permute-done | bytes 360480 | tf_op jit(solution)/shard_map/ppermute | solution.py:114
  61.9 1.8 collective-permute-done.15
  63.9 0.8 gather_fusion
  64.7 1.4 bitcast_select_fusion
  66.1 0.8 slice.97
  66.9 3.1 collective-permute-start
  71.7 0.9 broadcast_multiply_fusion
  72.5 0.6 copy-done.10
  73.1 10.3 %recurrence.1 = (f32[384,1024]{1,0:T(8,128)}, f32[384,1024]{1,0:T(8,128)}, f32[2,1024]{1,0:T(2,128)}) custom-call(bf16[384,1024]{1,0:T(8,128)(2,1)} %x.1, bf16[3,1024]{1,0:T(4,128)(2,1)} %copy-done.10, bf16[384,1024]{1,0:T(8,128)(2,1)} %gate.1, f32[4,1024]{1,0:T(4,128)} %taps.1, bf16[8,128,128]{2,1,0:T(8,128)(2,1)} %get-tuple-element.26.wa, ...), custom_call_target="tpu_custom_call" | custom-call | tf_op jit(solution)/shard_map/recurrence/pallas_call | solution.py:84
  83.5 0.9 collective-permute-start.1
  84.4 0.6 collective-permute-start.2
  85.0 0.9 collective-permute-start.3
  85.9 1.6 collective-permute-done.1
  87.9 0.6 collective-permute-done.3
  88.5 0.8 slice_multiply_fusion.5
  89.3 1.4 collective-permute-start.4
  90.7 1.5 collective-permute-start.5
  92.8 1.2 collective-permute-done.5
  93.9 2.1 collective-permute-done.6
  96.1 2.0 collective-permute-start.8
  98.1 0.8 collective-permute-start.9
  99.0 0.6 collective-permute-done.8
  99.6 1.4 collective-permute-done.9
  101.1 5.0 %convolution_convert_fusion.4 = bf16[384,2048]{1,0:T(8,128)(2,1)S(1)} fusion(bf16[1024,2048]{1,0:T(8,128)(2,1)} %param.23, f32[384,1024]{1,0:T(8,128)} %get-tuple-element.8, f32[384,1024]{1,0:T(8,128)} %get-tuple-element.9, f32[1024]{0:T(1024)S(1)} %bitcast.83), kind=kOutput, calls=%fused_computation.6 | convolution fusion | flops 1612578816 | bytes 8916992 | tf_op jit(solution)/shard_map/dot_general | solution.py:203
  106.1 6.0 %collective-permute-start.10 = (bf16[192,2048]{1,0:T(8,128)(2,1)S(1)}, bf16[192,2048]{1,0:T(8,128)(2,1)S(1)}, u32[]{:S(2)}, u32[]{:S(2)}) collective-permute-start(bf16[192,2048]{1,0:T(8,128)(2,1)S(1)} %dynamic-slice_bitcast_fusion), channel_id=1, source_target_pairs={{0,1},{1,0},{2,3},{3,2},{4,5},{5,4},{6,7},{7,6},{8,9},{9,8},{10,11... | collective-permute-start | bytes 2359304 | tf_op jit(solution)/shard_map/ppermute | solution.py:114
  112.2 1.9 collective-permute-done.10
  115.1 1.4 multiply_convert_fusion
  116.6 2.3 reshape.136
  118.9 1.3 copy.34
  120.2 1.6 reshape.137
  121.8 2.9 collective-permute-start.11
  124.7 1.5 collective-permute-start.25
  126.2 32.1 %collective-permute-done.11 = bf16[192,2048]{1,0:T(8,128)(2,1)} collective-permute-done((bf16[192,2048]{1,0:T(8,128)(2,1)S(1)}, bf16[192,2048]{1,0:T(8,128)(2,1)}, u32[]{:S(2)}, u32[]{:S(2)}) %collective-permute-start.11) | collective-permute-done | bytes 786464 | tf_op jit(solution)/shard_map/ppermute | solution.py:114
  158.2 0.9 collective-permute-start.12
  159.1 32.6 %collective-permute-done.21 = bf16[192,2048]{1,0:T(8,128)(2,1)} collective-permute-done((bf16[192,2048]{1,0:T(8,128)(2,1)S(1)}, bf16[192,2048]{1,0:T(8,128)(2,1)}, u32[]{:S(2)}, u32[]{:S(2)}) %collective-permute-start.21) | collective-permute-done | bytes 786464 | tf_op jit(solution)/shard_map/ppermute | solution.py:114
  192.2 0.6 collective-permute-done.25
  192.8 0.8 collective-permute-start.26
  193.6 5.6 %copy.32 = bf16[704,4,4,128]{3,2,1,0:T(4,128)(2,1)} copy(bf16[704,4,4,128]{3,0,1,2:T(8,128)(2,1)} %bitcast.67) | data formatting | bytes 5767168 | tf_op jit(solution)/shard_map/transpose | solution.py:187
  199.2 5.8 %reshape.141 = bf16[704,2048]{1,0:T(8,128)(2,1)} reshape(bf16[704,4,4,128]{3,2,1,0:T(4,128)(2,1)} %copy.32) | data formatting | bytes 5767168 | tf_op jit(solution)/shard_map/reshape | solution.py:187
  205.1 5.8 %fusion = f32[384,1408]{1,0:T(8,128)S(1)} fusion(bf16[2048,1408]{1,0:T(8,128)(2,1)} %all-gather.3.cloned.1.call-done, bf16[192,2048]{1,0:T(8,128)(2,1)} %collective-permute-done.12, bf16[192,2048]{1,0:T(8,128)(2,1)} %collective-permute-done.11), kind=kOutput, calls=%fused_computation.7 | convolution fusion | flops 2217738240 | bytes 9502720 | tf_op jit(solution)/shard_map/dot_general | solution.py:216
  210.9 1.5 convolution_convert_fusion.3
  212.6 1.0 copy-done.12
  213.6 4.0 %fusion.4 = f32[384,1408]{1,0:T(8,128)S(1)} fusion(bf16[2048,1408]{1,0:T(8,128)(2,1)S(1)} %copy-done.12, bf16[192,2048]{1,0:T(8,128)(2,1)} %collective-permute-done.22, bf16[192,2048]{1,0:T(8,128)(2,1)} %collective-permute-done.21), kind=kOutput, calls=%fused_computation.11 | convolution fusion | flops 2217738240 | bytes 9502720 | tf_op jit(solution)/shard_map/dot_general | solution.py:216
  217.5 1.5 convolution_convert_fusion.2
  219.2 4.0 %fusion.8 = f32[384,1408]{1,0:T(8,128)S(1)} fusion(bf16[2048,1408]{1,0:T(8,128)(2,1)S(1)} %copy-done.12, bf16[192,2048]{1,0:T(8,128)(2,1)} %collective-permute-done.26, bf16[192,2048]{1,0:T(8,128)(2,1)} %collective-permute-done.25), kind=kOutput, calls=%fused_computation.15 | convolution fusion | flops 2217738240 | bytes 9502720 | tf_op jit(solution)/shard_map/dot_general | solution.py:216
  223.2 1.5 convolution_convert_fusion.1
  225.3 3.7 %fusion.12 = f32[384,1408]{1,0:T(8,128)S(1)} fusion(bf16[2048,1408]{1,0:T(8,128)(2,1)S(1)} %copy-done.12, bf16[192,2048]{1,0:T(8,128)(2,1)} %collective-permute-done.29, bf16[192,2048]{1,0:T(8,128)(2,1)S(1)} %reshape.137), kind=kOutput, calls=%fused_computation.19 | convolution fusion | flops 2217738240 | bytes 9502720 | tf_op jit(solution)/shard_map/dot_general | solution.py:216
  229.0 1.5 convolution_convert_fusion
  231.4 2.9 collective-permute-start.24
  234.6 46.9 %collective-permute-done.20 = bf16[192,2048]{1,0:T(8,128)(2,1)S(1)} collective-permute-done((bf16[192,2048]{1,0:T(8,128)(2,1)S(1)}, bf16[192,2048]{1,0:T(8,128)(2,1)S(1)}, u32[]{:S(2)}, u32[]{:S(2)}) %collective-permute-start.20) | collective-permute-done | bytes 786464 | tf_op jit(solution)/shard_map/ppermute | solution.py:114
  281.5 19.4 %collective-permute-done.24 = bf16[192,2048]{1,0:T(8,128)(2,1)S(1)} collective-permute-done((bf16[192,2048]{1,0:T(8,128)(2,1)S(1)}, bf16[192,2048]{1,0:T(8,128)(2,1)S(1)}, u32[]{:S(2)}, u32[]{:S(2)}) %collective-permute-start.24) | collective-permute-done | bytes 786464 | tf_op jit(solution)/shard_map/ppermute | solution.py:114
  300.9 0.6 multiply_reduce_fusion
  301.6 2.3 add_convert_fusion
  (98 shorter events, 9.4 us)
Async XLA Ops:
  6.5 187.1 %all-gather.5.cloned.1.call-start = ((), (), s32[]{:S(2)}) async-start(), calls=%async_computation.1 | async-start | bytes 3604480 | tf_op jit(solution)/shard_map/all_gather | solution.py:186
  7.8 5.5 %collective-permute-start.16 = (bf16[704,128]{1,0:T(8,128)(2,1)S(1)}, bf16[704,128]{1,0:T(8,128)(2,1)S(1)}, u32[]{:S(2)}, u32[]{:S(2)}) collective-permute-start(bf16[704,128]{1,0:T(8,128)(2,1)S(1)} %get-tuple-element.22), channel_id=1, source_target_pairs={{0,8},{8,16},{16,24},{24,0},{1,9},{9,17},{17,25},{25,1},{2,10},{10... | collective-permute-start | bytes 540680 | tf_op jit(solution)/shard_map/ppermute | solution.py:114
  9.1 14.8 %collective-permute-start.17 = (bf16[704,128]{1,0:T(8,128)(2,1)S(1)}, bf16[704,128]{1,0:T(8,128)(2,1)S(1)}, u32[]{:S(2)}, u32[]{:S(2)}) collective-permute-start(bf16[704,128]{1,0:T(8,128)(2,1)S(1)} %get-tuple-element.21), channel_id=1, source_target_pairs={{0,16},{8,24},{16,0},{24,8},{1,17},{9,25},{17,1},{25,9},{2,18},{10... | collective-permute-start | bytes 540680 | tf_op jit(solution)/shard_map/ppermute | solution.py:114
  10.2 16.5 %collective-permute-start.18 = (bf16[704,128]{1,0:T(8,128)(2,1)S(1)}, bf16[704,128]{1,0:T(8,128)(2,1)S(1)}, u32[]{:S(2)}, u32[]{:S(2)}) collective-permute-start(bf16[704,128]{1,0:T(8,128)(2,1)S(1)} %get-tuple-element.20), channel_id=1, source_target_pairs={{0,24},{8,0},{16,8},{24,16},{1,25},{9,1},{17,9},{25,17},{2,26},{10... | collective-permute-start | bytes 540680 | tf_op jit(solution)/shard_map/ppermute | solution.py:114
  26.8 3.0 copy-start.3
  27.5 2.7 copy-start.4
  29.8 175.3 %all-gather.3.cloned.1.call-start = ((), (), s32[]{:S(2)}) async-start(), calls=%async_computation | async-start | bytes 7208960 | tf_op jit(solution)/shard_map/all_gather | solution.py:184
  31.1 9.6 %collective-permute-start.13 = (bf16[128,1408]{1,0:T(8,128)(2,1)S(1)}, bf16[128,1408]{1,0:T(8,128)(2,1)S(1)}, u32[]{:S(2)}, u32[]{:S(2)}) collective-permute-start(bf16[128,1408]{1,0:T(8,128)(2,1)S(1)} %bitcast.72), channel_id=1, source_target_pairs={{0,8},{8,16},{16,24},{24,0},{1,9},{9,17},{17,25},{25,1},{2,10},{10... | collective-permute-start | bytes 1081352 | tf_op jit(solution)/shard_map/ppermute | solution.py:114
  31.4 30.5 %collective-permute-start.14 = (bf16[128,1408]{1,0:T(8,128)(2,1)S(1)}, bf16[128,1408]{1,0:T(8,128)(2,1)S(1)}, u32[]{:S(2)}, u32[]{:S(2)}) collective-permute-start(bf16[128,1408]{1,0:T(8,128)(2,1)S(1)} %bitcast.73), channel_id=1, source_target_pairs={{0,16},{8,24},{16,0},{24,8},{1,17},{9,25},{17,1},{25,9},{2,18},{10... | collective-permute-start | bytes 1081352 | tf_op jit(solution)/shard_map/ppermute | solution.py:114
  32.0 31.7 %collective-permute-start.15 = (bf16[128,1408]{1,0:T(8,128)(2,1)S(1)}, bf16[128,1408]{1,0:T(8,128)(2,1)S(1)}, u32[]{:S(2)}, u32[]{:S(2)}) collective-permute-start(bf16[128,1408]{1,0:T(8,128)(2,1)S(1)} %bitcast.74), channel_id=1, source_target_pairs={{0,24},{8,0},{16,8},{24,16},{1,25},{9,1},{17,9},{25,17},{2,26},{10... | collective-permute-start | bytes 1081352 | tf_op jit(solution)/shard_map/ppermute | solution.py:114
  64.7 5.3 %copy-start.5 = (bf16[16,64,64]{2,1,0:T(8,128)(2,1)S(1)}, bf16[16,64,64]{2,1,0:T(8,128)(2,1)}, u32[]{:S(2)}) copy-start(bf16[16,64,64]{2,1,0:T(8,128)(2,1)} %param.19) | copy-start | bytes 393220
  66.1 4.6 %copy-start.6 = (bf16[16,64,64]{2,1,0:T(8,128)(2,1)S(1)}, bf16[16,64,64]{2,1,0:T(8,128)(2,1)}, u32[]{:S(2)}) copy-start(bf16[16,64,64]{2,1,0:T(8,128)(2,1)} %param.20) | copy-start | bytes 393220
  66.9 5.6 %collective-permute-start = (bf16[3,1024]{1,0:T(4,128)(2,1)S(1)}, bf16[3,1024]{1,0:T(4,128)(2,1)S(1)}, u32[]{:S(2)}, u32[]{:S(2)}) collective-permute-start(bf16[3,1024]{1,0:T(4,128)(2,1)S(1)} %slice.97), channel_id=1, source_target_pairs={{0,2},{2,4},{4,6},{6,8},{8,10},{10,12},{12,14},{14,16},{16,18},{18... | collective-permute-start | bytes 18440 | tf_op jit(solution)/shard_map/ppermute | solution.py:190
  72.5 0.6 copy-start.10
  73.1 15.3 %copy-start.8 = (f32[2,1024]{1,0:T(2,128)S(1)}, f32[2,1024]{1,0:T(2,128)}, u32[]{:S(2)}) copy-start(f32[2,1024]{1,0:T(2,128)} %constant.123.clone.1) | copy-start | bytes 24580
  83.5 4.0 %collective-permute-start.1 = (f32[2,1024]{1,0:T(2,128)}, f32[2,1024]{1,0:T(2,128)S(1)}, u32[]{:S(2)}, u32[]{:S(2)}) collective-permute-start(f32[2,1024]{1,0:T(2,128)} %get-tuple-element.10), channel_id=1, source_target_pairs={{0,6},{2,0},{4,2},{6,4},{1,7},{3,1},{5,3},{7,5},{8,14},{10,8},{12,... | collective-permute-start | bytes 24584 | tf_op jit(solution)/shard_map/ppermute | solution.py:114
  84.4 3.5 %collective-permute-start.2 = (f32[2,1024]{1,0:T(2,128)}, f32[2,1024]{1,0:T(2,128)S(1)}, u32[]{:S(2)}, u32[]{:S(2)}) collective-permute-start(f32[2,1024]{1,0:T(2,128)} %get-tuple-element.10), channel_id=1, source_target_pairs={{0,4},{2,6},{4,0},{6,2},{1,5},{3,7},{5,1},{7,3},{8,12},{10,14},{12... | collective-permute-start | bytes 24584 | tf_op jit(solution)/shard_map/ppermute | solution.py:114
  85.0 3.5 %collective-permute-start.3 = (f32[2,1024]{1,0:T(2,128)}, f32[2,1024]{1,0:T(2,128)S(1)}, u32[]{:S(2)}, u32[]{:S(2)}) collective-permute-start(f32[2,1024]{1,0:T(2,128)} %get-tuple-element.10), channel_id=1, source_target_pairs={{0,2},{2,4},{4,6},{6,0},{1,3},{3,5},{5,7},{7,1},{8,10},{10,12},{12... | collective-permute-start | bytes 24584 | tf_op jit(solution)/shard_map/ppermute | solution.py:114
  89.3 3.5 %collective-permute-start.4 = (f32[2,1024]{1,0:T(2,128)S(1)}, f32[2,1024]{1,0:T(2,128)S(1)}, u32[]{:S(2)}, u32[]{:S(2)}) collective-permute-start(f32[2,1024]{1,0:T(2,128)S(1)} %maximum_select_fusion), channel_id=1, source_target_pairs={{0,2},{2,4},{4,6},{6,0},{1,3},{3,5},{5,7},{7,1},{8,10},{10,12},{12... | collective-permute-start | bytes 24584 | tf_op jit(solution)/shard_map/ppermute | solution.py:114
  90.7 3.2 %collective-permute-start.5 = (f32[2,1024]{1,0:T(2,128)S(1)}, f32[2,1024]{1,0:T(2,128)S(1)}, u32[]{:S(2)}, u32[]{:S(2)}) collective-permute-start(f32[2,1024]{1,0:T(2,128)S(1)} %maximum_select_fusion), channel_id=1, source_target_pairs={{0,4},{2,6},{4,0},{6,2},{1,5},{3,7},{5,1},{7,3},{8,12},{10,14},{12... | collective-permute-start | bytes 24584 | tf_op jit(solution)/shard_map/ppermute | solution.py:114
  92.2 3.8 %collective-permute-start.6 = (f32[2,1024]{1,0:T(2,128)S(1)}, f32[2,1024]{1,0:T(2,128)S(1)}, u32[]{:S(2)}, u32[]{:S(2)}) collective-permute-start(f32[2,1024]{1,0:T(2,128)S(1)} %maximum_select_fusion), channel_id=1, source_target_pairs={{0,6},{2,0},{4,2},{6,4},{1,7},{3,1},{5,3},{7,5},{8,14},{10,8},{12,... | collective-permute-start | bytes 24584 | tf_op jit(solution)/shard_map/ppermute | solution.py:114
  96.1 3.0 collective-permute-start.7
  96.1 3.5 %collective-permute-start.8 = (f32[2,1024]{1,0:T(2,128)S(1)}, f32[2,1024]{1,0:T(2,128)S(1)}, u32[]{:S(2)}, u32[]{:S(2)}) collective-permute-start(f32[2,1024]{1,0:T(2,128)S(1)} %add_add_fusion.1), channel_id=1, source_target_pairs={{0,16},{8,24},{16,0},{24,8},{1,17},{9,25},{17,1},{25,9},{2,18},{10... | collective-permute-start | bytes 24584 | tf_op jit(solution)/shard_map/ppermute | solution.py:114
  98.1 2.9 collective-permute-start.9
  106.0 8.4 %copy-start.7 = (f32[2048]{0:T(1024)S(1)}, f32[2048]{0:T(1024)}, u32[]{:S(2)}) copy-start(f32[2048]{0:T(1024)} %param.24) | copy-start | bytes 24580
  106.1 8.0 %collective-permute-start.10 = (bf16[192,2048]{1,0:T(8,128)(2,1)S(1)}, bf16[192,2048]{1,0:T(8,128)(2,1)S(1)}, u32[]{:S(2)}, u32[]{:S(2)}) collective-permute-start(bf16[192,2048]{1,0:T(8,128)(2,1)S(1)} %dynamic-slice_bitcast_fusion), channel_id=1, source_target_pairs={{0,1},{1,0},{2,3},{3,2},{4,5},{5,4},{6,7},{7,6},{8,9},{9,8},{10,11... | collective-permute-start | bytes 2359304 | tf_op jit(solution)/shard_map/ppermute | solution.py:114
  112.2 2.3 copy-start
  114.4 0.7 copy-start.9
  121.8 36.4 %collective-permute-start.11 = (bf16[192,2048]{1,0:T(8,128)(2,1)S(1)}, bf16[192,2048]{1,0:T(8,128)(2,1)}, u32[]{:S(2)}, u32[]{:S(2)}) collective-permute-start(bf16[192,2048]{1,0:T(8,128)(2,1)S(1)} %reshape.137), channel_id=1, source_target_pairs={{0,16},{8,24},{16,0},{24,8},{1,17},{9,25},{17,1},{25,9},{2,18},{10... | collective-permute-start | bytes 2359304 | tf_op jit(solution)/shard_map/ppermute | solution.py:114
  124.7 67.0 %collective-permute-start.21 = (bf16[192,2048]{1,0:T(8,128)(2,1)S(1)}, bf16[192,2048]{1,0:T(8,128)(2,1)}, u32[]{:S(2)}, u32[]{:S(2)}) collective-permute-start(bf16[192,2048]{1,0:T(8,128)(2,1)S(1)} %reshape.137), channel_id=1, source_target_pairs={{0,8},{8,16},{16,24},{24,0},{1,9},{9,17},{17,25},{25,1},{2,10},{10... | collective-permute-start | bytes 2359304 | tf_op jit(solution)/shard_map/ppermute | solution.py:114
  124.7 68.1 %collective-permute-start.25 = (bf16[192,2048]{1,0:T(8,128)(2,1)S(1)}, bf16[192,2048]{1,0:T(8,128)(2,1)}, u32[]{:S(2)}, u32[]{:S(2)}) collective-permute-start(bf16[192,2048]{1,0:T(8,128)(2,1)S(1)} %reshape.137), channel_id=1, source_target_pairs={{0,24},{8,0},{16,8},{24,16},{1,25},{9,1},{17,9},{25,17},{2,26},{10... | collective-permute-start | bytes 2359304 | tf_op jit(solution)/shard_map/ppermute | solution.py:114
  158.2 46.8 %collective-permute-start.12 = (bf16[192,2048]{1,0:T(8,128)(2,1)}, bf16[192,2048]{1,0:T(8,128)(2,1)}, u32[]{:S(2)}, u32[]{:S(2)}) collective-permute-start(bf16[192,2048]{1,0:T(8,128)(2,1)} %collective-permute-done.11), channel_id=1, source_target_pairs={{0,1},{1,0},{2,3},{3,2},{4,5},{5,4},{6,7},{7,6},{8,9},{9,8},{10,11... | collective-permute-start | bytes 2359304 | tf_op jit(solution)/shard_map/ppermute | solution.py:114
  159.1 66.2 %collective-permute-start.29 = (bf16[192,2048]{1,0:T(8,128)(2,1)S(1)}, bf16[192,2048]{1,0:T(8,128)(2,1)}, u32[]{:S(2)}, u32[]{:S(2)}) collective-permute-start(bf16[192,2048]{1,0:T(8,128)(2,1)S(1)} %reshape.137), channel_id=1, source_target_pairs={{0,1},{1,0},{2,3},{3,2},{4,5},{5,4},{6,7},{7,6},{8,9},{9,8},{10,11... | collective-permute-start | bytes 2359304 | tf_op jit(solution)/shard_map/ppermute | solution.py:114
  191.7 20.9 %collective-permute-start.22 = (bf16[192,2048]{1,0:T(8,128)(2,1)}, bf16[192,2048]{1,0:T(8,128)(2,1)}, u32[]{:S(2)}, u32[]{:S(2)}) collective-permute-start(bf16[192,2048]{1,0:T(8,128)(2,1)} %collective-permute-done.21), channel_id=1, source_target_pairs={{0,1},{1,0},{2,3},{3,2},{4,5},{5,4},{6,7},{7,6},{8,9},{9,8},{10,11... | collective-permute-start | bytes 2359304 | tf_op jit(solution)/shard_map/ppermute | solution.py:114
  192.8 26.4 %collective-permute-start.26 = (bf16[192,2048]{1,0:T(8,128)(2,1)}, bf16[192,2048]{1,0:T(8,128)(2,1)}, u32[]{:S(2)}, u32[]{:S(2)}) collective-permute-start(bf16[192,2048]{1,0:T(8,128)(2,1)} %collective-permute-done.25), channel_id=1, source_target_pairs={{0,1},{1,0},{2,3},{3,2},{4,5},{5,4},{6,7},{7,6},{8,9},{9,8},{10,11... | collective-permute-start | bytes 2359304 | tf_op jit(solution)/shard_map/ppermute | solution.py:114
  205.1 5.9 %copy-start.2 = (bf16[704,2048]{1,0:T(8,128)(2,1)S(1)}, bf16[704,2048]{1,0:T(8,128)(2,1)}, u32[]{:S(2)}) copy-start(bf16[704,2048]{1,0:T(8,128)(2,1)} %reshape.141) | copy-start | bytes 8650756
  210.9 2.6 copy-start.12
  212.5 18.2 %collective-permute-start.19 = (bf16[192,2048]{1,0:T(8,128)(2,1)S(1)}, bf16[192,2048]{1,0:T(8,128)(2,1)S(1)}, u32[]{:S(2)}, u32[]{:S(2)}) collective-permute-start(bf16[192,2048]{1,0:T(8,128)(2,1)S(1)} %slice.147), channel_id=1, source_target_pairs={{0,1},{1,0},{2,3},{3,2},{4,5},{5,4},{6,7},{7,6},{8,9},{9,8},{10,11... | collective-permute-start | bytes 2359304 | tf_op jit(solution)/shard_map/ppermute | solution.py:114
  219.1 12.0 %collective-permute-start.23 = (bf16[192,2048]{1,0:T(8,128)(2,1)S(1)}, bf16[192,2048]{1,0:T(8,128)(2,1)S(1)}, u32[]{:S(2)}, u32[]{:S(2)}) collective-permute-start(bf16[192,2048]{1,0:T(8,128)(2,1)S(1)} %slice.151), channel_id=1, source_target_pairs={{0,1},{1,0},{2,3},{3,2},{4,5},{5,4},{6,7},{7,6},{8,9},{9,8},{10,11... | collective-permute-start | bytes 2359304 | tf_op jit(solution)/shard_map/ppermute | solution.py:114
  224.8 9.5 %collective-permute-start.27 = (bf16[192,2048]{1,0:T(8,128)(2,1)S(1)}, bf16[192,2048]{1,0:T(8,128)(2,1)S(1)}, u32[]{:S(2)}, u32[]{:S(2)}) collective-permute-start(bf16[192,2048]{1,0:T(8,128)(2,1)S(1)} %slice.155), channel_id=1, source_target_pairs={{0,1},{1,0},{2,3},{3,2},{4,5},{5,4},{6,7},{7,6},{8,9},{9,8},{10,11... | collective-permute-start | bytes 2359304 | tf_op jit(solution)/shard_map/ppermute | solution.py:114
  230.6 3.9 %collective-permute-start.30 = (bf16[192,2048]{1,0:T(8,128)(2,1)S(1)}, bf16[192,2048]{1,0:T(8,128)(2,1)S(1)}, u32[]{:S(2)}, u32[]{:S(2)}) collective-permute-start(bf16[192,2048]{1,0:T(8,128)(2,1)S(1)} %slice.159), channel_id=1, source_target_pairs={{0,1},{1,0},{2,3},{3,2},{4,5},{5,4},{6,7},{7,6},{8,9},{9,8},{10,11... | collective-permute-start | bytes 2359304 | tf_op jit(solution)/shard_map/ppermute | solution.py:114
  231.0 50.5 %collective-permute-start.20 = (bf16[192,2048]{1,0:T(8,128)(2,1)S(1)}, bf16[192,2048]{1,0:T(8,128)(2,1)S(1)}, u32[]{:S(2)}, u32[]{:S(2)}) collective-permute-start(bf16[192,2048]{1,0:T(8,128)(2,1)S(1)} %add_convert_fusion.3), channel_id=1, source_target_pairs={{0,16},{8,24},{16,0},{24,8},{1,17},{9,25},{17,1},{25,9},{2,18},{10... | collective-permute-start | bytes 2359304 | tf_op jit(solution)/shard_map/ppermute | solution.py:114
  231.4 69.6 %collective-permute-start.24 = (bf16[192,2048]{1,0:T(8,128)(2,1)S(1)}, bf16[192,2048]{1,0:T(8,128)(2,1)S(1)}, u32[]{:S(2)}, u32[]{:S(2)}) collective-permute-start(bf16[192,2048]{1,0:T(8,128)(2,1)S(1)} %add_convert_fusion.2), channel_id=1, source_target_pairs={{0,24},{8,0},{16,8},{24,16},{1,25},{9,1},{17,9},{25,17},{2,26},{10... | collective-permute-start | bytes 2359304 | tf_op jit(solution)/shard_map/ppermute | solution.py:114
  234.5 67.1 %copy-start.1 = (bf16[384,2048]{1,0:T(8,128)(2,1)S(1)}, bf16[384,2048]{1,0:T(8,128)(2,1)}, u32[]{:S(2)}) copy-start(bf16[384,2048]{1,0:T(8,128)(2,1)} %param.15) | copy-start | bytes 4718596
  234.5 67.1 %copy-start.11 = (f32[2048]{0:T(1024)S(1)}, f32[2048]{0:T(1024)}, u32[]{:S(2)}) copy-start(f32[2048]{0:T(1024)} %param.29) | copy-start | bytes 24580
  234.5 66.4 %collective-permute-start.28 = (bf16[192,2048]{1,0:T(8,128)(2,1)S(1)}, bf16[192,2048]{1,0:T(8,128)(2,1)S(1)}, u32[]{:S(2)}, u32[]{:S(2)}) collective-permute-start(bf16[192,2048]{1,0:T(8,128)(2,1)S(1)} %add_convert_fusion.1), channel_id=1, source_target_pairs={{0,8},{8,16},{16,24},{24,0},{1,9},{9,17},{17,25},{25,1},{2,10},{10... | collective-permute-start | bytes 2359304 | tf_op jit(solution)/shard_map/ppermute | solution.py:114
Sparse Core Ops, SparseCore 0:
  29.9 41.4 all-gather.4
  73.3 66.3 all-gather.2
